TPU v7x, 512 devices: a whole 4x4x16 slice. The times are simulated.
512 devices in a mesh: sp: 16 (over z), fs: 4 (over y), tp: 8 (over x, core).
Axes of the slice: x: 4, y: 4, z: 16, core: 2. Of those that a mesh axis runs over, the one named last changes fastest.
Arguments:
- tokens: bfloat16 [4, 4096, 2048], P('fs', ('sp', 'tp')), may hold values from -6 to 6
- query_weight: bfloat16 [2048, 2048], P(('sp', 'fs'), 'tp'), may hold values from -0.125 to 0.125
- forget_weight: bfloat16 [2048, 2048], P(('sp', 'fs'), 'tp'), may hold values from -0.125 to 0.125
- value_weight: bfloat16 [2048, 2048], P(('sp', 'fs'), 'tp'), may hold values from -0.125 to 0.125
- convolution_gate_weight: bfloat16 [2048, 1024], P(('sp', 'fs'), 'tp'), may hold values from -0.125 to 0.125
- convolution_multiplier_weight: bfloat16 [2048, 1024], P(('sp', 'fs'), 'tp'), may hold values from -0.125 to 0.125
- convolution_input_weight: bfloat16 [2048, 1024], P(('sp', 'fs'), 'tp'), may hold values from -0.125 to 0.125
- gate_headroom: float32 [2048], P('tp'), may hold values from 2.4414063e-05 to 0.06
- added_log_rate: float32 [4, 16, 4096], P('fs', 'tp', 'sp'), may hold values from -1.6 to 0
- initial_state: float32 [4, 16, 128, 128], P('fs', 'tp'), may hold values from -0.25 to 0.25
- head_norm_gain: float32 [2048], P('tp'), may hold values from 0.1 to 1.9
- convolution_taps: float32 [3, 1024], P(None, 'tp'), may hold values from -3.5 to 3.5
- convolution_bias: float32 [1024], P('tp'), may hold values from -4 to 4
- recurrence_output_weight: bfloat16 [2048, 2048], P('tp', ('sp', 'fs')), may hold values from -0.109375 to 0.109375
- convolution_output_weight: bfloat16 [1024, 2048], P('tp', ('sp', 'fs')), may hold values from -0.109375 to 0.109375
Outputs:
- mixed: bfloat16 [4, 4096, 2048], P('fs', ('sp', 'tp'))
All inputs are finite; a program needn't handle non-finite values.
Results may differ from a plain program's by a relative error of at most 0.018.
Values may be sent and summed in bfloat16 or wider, within the bound.
A program may use at most 64 MiB of HBM per device.

v0:
```python
import jax
import jax.numpy as jnp
from jax import lax
from jax.sharding import PartitionSpec as P

DK = 128
KW = 3
BLOCK_POSITIONS = 64


def gather_turned(arrays, axis, dims):
    turned = [jnp.moveaxis(a, dim, 0) for a, dim in zip(arrays, dims)]
    widths = [t[0].size for t in turned]
    both = jnp.concatenate([t.reshape(-1, w) for t, w in zip(turned, widths)], axis=1)
    result = lax.all_gather(both, axis, axis=0, tiled=True)
    parts = jnp.split(result, [sum(widths[:k]) for k in range(1, len(widths))], axis=1)
    return tuple(
        (
            jnp.moveaxis(b.reshape(-1, *t.shape[1:]), 0, dim)
            for b, t, dim in zip(parts, turned, dims)
        )
    )


def copy_for_each(value, axis):
    copies = jnp.broadcast_to(value, (lax.axis_size(axis), *value.shape))
    return lax.all_to_all(copies, axis, split_axis=0, concat_axis=0, tiled=True)


def in_order(parts, dim):
    parts = jnp.moveaxis(parts, 0, dim)
    dims = parts.shape
    return parts.reshape(*dims[:dim], dims[dim] * dims[dim + 1], *dims[dim + 2 :])


def gather_directly(value, axis, dim):
    parts = copy_for_each(value, axis)
    return in_order(parts, dim)


def carried_in(part, axis, combine, identity):
    place = lax.axis_index(axis)
    gathered = jax.tree.map(lambda a: lax.all_gather(a, axis), part)
    state = jax.tree.map(lambda a, e: jnp.zeros_like(a) + jnp.asarray(e, a.dtype), part, identity)

    def one(hop, state):
        return combine(
            state, jax.tree.map(lambda a: lax.dynamic_index_in_dim(a, hop, 0, False), gathered)
        )

    return lax.fori_loop(0, place, one, state)


def from_behind(block, axis, distance):
    devices = range(lax.axis_size(axis))
    route = [(i - distance, i) for i in devices if i - distance in devices]
    return lax.ppermute(block, axis, route)


def in_blocks(value, dim, peers):
    before, after = (value.shape[:dim], value.shape[dim + 1 :])
    return jnp.moveaxis(value.reshape(*before, peers, -1, *after), dim, 0)


def summed_on_arrival(value, axis, dim):
    parts = in_blocks(value, dim, lax.axis_size(axis))
    arrived = lax.all_to_all(parts, axis, split_axis=0, concat_axis=0, tiled=True)
    return arrived.astype(jnp.float32).sum(axis=0)


def to_blocks(values, number_of_heads):
    number_of_blocks = values.shape[0] // BLOCK_POSITIONS
    return jnp.transpose(
        values.reshape(number_of_blocks, BLOCK_POSITIONS, number_of_heads, DK), (2, 0, 1, 3)
    )


def within_block_recurrence(
    query_vectors, forget_logits, value_vectors, gate_headroom, extra_rates
):
    number_of_heads = extra_rates.shape[0]
    number_of_blocks = query_vectors.shape[0] // BLOCK_POSITIONS
    query_scaled = to_blocks(query_vectors.astype(jnp.float32), number_of_heads) * DK ** (-0.5)
    gated_key = to_blocks(
        gate_headroom[None, :] * jax.nn.sigmoid(-forget_logits.astype(jnp.float32)), number_of_heads
    )
    forget_log_rate = (
        jnp.log1p(-gated_key)
        + extra_rates.reshape(number_of_heads, number_of_blocks, BLOCK_POSITIONS)[..., None]
    )
    values = to_blocks(value_vectors.astype(jnp.float32), number_of_heads)
    cumulative = jnp.cumsum(forget_log_rate, axis=2)
    query_decayed = query_scaled * jnp.exp(cumulative)
    key_decayed = gated_key * jnp.exp(-cumulative)
    scores = jnp.einsum("hnik,hnjk->hnij", query_decayed, key_decayed)
    causal = jnp.tril(jnp.ones((BLOCK_POSITIONS, BLOCK_POSITIONS), dtype=bool))
    scores = jnp.where(causal, scores, 0.0)
    within = jnp.einsum("hnij,hnjv->hniv", scores, values)
    final_log = cumulative[:, :, -1, :]
    contrib = jnp.einsum(
        "hnck,hncv->hnkv", gated_key * jnp.exp(final_log[:, :, None, :] - cumulative), values
    )
    decays = jnp.exp(final_log)

    def advance(current, block_pair):
        return (block_pair[0][..., None] * current + block_pair[1], current)

    empty_state = jnp.zeros((number_of_heads, DK, DK), jnp.float32)
    local_total, entering = lax.scan(
        advance, empty_state, (jnp.moveaxis(decays, 1, 0), jnp.moveaxis(contrib, 1, 0))
    )
    entering = jnp.moveaxis(entering, 0, 1)
    before = jnp.exp(jnp.cumsum(final_log, axis=1) - final_log)
    device_decay = jnp.exp(jnp.sum(final_log, axis=1))
    return (query_decayed, within, entering, before, device_decay, local_total)


def finish(query_decayed, within, entering, before, carried, head_norm_gain):
    number_of_heads = query_decayed.shape[0]
    states = entering + before[..., None] * carried[:, None]
    carried_term = jnp.einsum("hnck,hnkv->hncv", query_decayed, states)
    length = query_decayed.shape[1] * BLOCK_POSITIONS
    recurrence_unnormed = jnp.transpose(within + carried_term, (1, 2, 0, 3)).reshape(
        length, number_of_heads, DK
    )
    mean_square = jnp.mean(recurrence_unnormed * recurrence_unnormed, axis=-1, keepdims=True)
    rec_out = (
        recurrence_unnormed
        * lax.rsqrt(mean_square + 1e-06)
        * head_norm_gain.reshape(number_of_heads, DK)
    )
    return rec_out.reshape(length, number_of_heads * DK).astype(jnp.bfloat16)


def chain_combine(earlier_part, later_part):
    return (
        earlier_part[0] * later_part[0],
        later_part[0][..., None] * earlier_part[1] + later_part[1],
    )


def shards(
    tokens,
    query_weight,
    forget_weight,
    value_weight,
    convolution_gate_weight,
    convolution_multiplier_weight,
    convolution_input_weight,
    gate_headroom,
    added_log_rate,
    initial_state,
    head_norm_gain,
    convolution_taps,
    convolution_bias,
    recurrence_output_weight,
    convolution_output_weight,
):
    own_rows = tokens[0]
    gathered = gather_turned(
        (
            query_weight,
            forget_weight,
            value_weight,
            convolution_gate_weight,
            convolution_multiplier_weight,
            convolution_input_weight,
            recurrence_output_weight,
            convolution_output_weight,
        ),
        ("sp", "fs"),
        (0, 0, 0, 0, 0, 0, 1, 1),
    )
    in_weights = gathered[:6]
    out_rec = gathered[6]
    out_conv = gathered[7]
    block_rows = gather_directly(own_rows, "tp", 0)
    projected = jnp.concatenate(
        [
            jnp.dot(block_rows, weight, preferred_element_type=jnp.float32).astype(jnp.bfloat16)
            for weight in in_weights
        ],
        axis=1,
    )
    rec_width = query_weight.shape[1]
    conv_width = convolution_gate_weight.shape[1]
    query_vectors = projected[:, :rec_width]
    forget_logits = projected[:, rec_width : 2 * rec_width]
    value_vectors = projected[:, 2 * rec_width : 3 * rec_width]
    conv_base = 3 * rec_width
    conv_gate = projected[:, conv_base : conv_base + conv_width]
    conv_mult = projected[:, conv_base + conv_width : conv_base + 2 * conv_width]
    conv_input = projected[:, conv_base + 2 * conv_width : conv_base + 3 * conv_width]
    query_decayed, within, entering, before, device_decay, local_total = within_block_recurrence(
        query_vectors, forget_logits, value_vectors, gate_headroom, added_log_rate[0]
    )
    conv_prod = conv_mult.astype(jnp.float32) * conv_input.astype(jnp.float32)
    length = conv_prod.shape[0]
    tail_rows = conv_prod[length - (KW - 1) :]
    unit_decay = jnp.ones_like(device_decay)
    empty_state = jnp.zeros_like(local_total)
    prior_decay, prior_state = carried_in(
        (device_decay, local_total), "sp", chain_combine, (unit_decay, empty_state)
    )
    prior_rows = from_behind(tail_rows, "sp", 1)
    carried = prior_decay[..., None] * initial_state[0] + prior_state
    rec_out = finish(query_decayed, within, entering, before, carried, head_norm_gain)
    extended = jnp.concatenate([prior_rows, conv_prod], axis=0)
    conv_y = jnp.broadcast_to(convolution_bias[None, :], conv_prod.shape)
    for j in range(KW):
        conv_y = conv_y + convolution_taps[j][None, :] * extended[j : j + length]
    conv_out = (conv_gate.astype(jnp.float32) * conv_y).astype(jnp.bfloat16)
    mixed = summed_on_arrival(
        (
            jnp.dot(rec_out, out_rec, preferred_element_type=jnp.float32)
            + jnp.dot(conv_out, out_conv, preferred_element_type=jnp.float32)
        ).astype(jnp.bfloat16),
        "tp",
        0,
    )
    return mixed.astype(jnp.bfloat16)[None]


def solution(mesh):
    in_specs = (
        P("fs", ("sp", "tp"), None),
        P(("sp", "fs"), "tp"),
        P(("sp", "fs"), "tp"),
        P(("sp", "fs"), "tp"),
        P(("sp", "fs"), "tp"),
        P(("sp", "fs"), "tp"),
        P(("sp", "fs"), "tp"),
        P("tp"),
        P("fs", "tp", "sp"),
        P("fs", "tp", None, None),
        P("tp"),
        P(None, "tp"),
        P("tp"),
        P("tp", ("sp", "fs")),
        P("tp", ("sp", "fs")),
    )
    out_specs = P("fs", ("sp", "tp"), None)
    return jax.shard_map(shards, mesh=mesh, in_specs=in_specs, out_specs=out_specs, check_vma=False)
```

profile of v0, /device:TPU:488, one launch (start us, length us, event | category | flops | bytes accessed | tf_op | source)
XLA Modules:
  0.0 286.8 jit_solution(150869934221793700)
XLA Ops:
  12.9 2.0 broadcast_in_dim.41
  14.9 4.3 %all-to-all-start = ((bf16[8,32,2048]{2,1,0:T(8,128)(2,1)}), bf16[8,32,2048]{2,1,0:T(8,128)(2,1)S(1)}, u32[]{:S(2)}, u32[]{:S(2)}) async-start(bf16[8,32,2048]{2,1,0:T(8,128)(2,1)} %broadcast_in_dim.41), calls=%async_computation | async-start | bytes 2097152 | tf_op jit(solution)/shard_map/all_to_all | solution.py:27
  20.0 15.1 %all-to-all-done = bf16[8,32,2048]{2,1,0:T(8,128)(2,1)S(1)} async-done(((bf16[8,32,2048]{2,1,0:T(8,128)(2,1)}), bf16[8,32,2048]{2,1,0:T(8,128)(2,1)S(1)}, u32[]{:S(2)}, u32[]{:S(2)}) %all-to-all-start) | async-done | bytes 1048608 | tf_op jit(solution)/shard_map/all_to_all | solution.py:27
  35.2 125.2 %all-gather.6.cloned.1.call-done = bf16[2048,1536]{1,0:T(8,128)(2,1)} async-done(((bf16[32,1536]{1,0:T(8,128)(2,1)}), bf16[2048,1536]{1,0:T(8,128)(2,1)}) %all-gather.6.cloned.1.call-update) | async-done | bytes 6291472 | tf_op jit(solution)/shard_map/all_gather | solution.py:15
  160.4 1.7 fusion.8
  163.0 1.7 fusion.12
  166.7 1.7 fusion.11
  168.8 1.5 fusion.16
  170.4 1.5 fusion.15
  172.0 1.3 collective-permute-start
  173.3 27.9 %all-gather.2 = f32[16,2,128]{2,1,0:T(2,128)S(1)} all-gather(f32[1,2,128]{2,1,0:T(2,128)S(1)} %exponential_bitcast_fusion.1), channel_id=2, replica_groups=mesh['sp'=16,'fs'=4,'tp'=8] {'sp'}, dimensions={0}, use_global_device_ids=true | all-gather | bytes 17408 | tf_op jit(solution)/shard_map/all_gather | solution.py:43
  201.5 34.2 %all-gather.8.cloned.1.call-done = f32[32,128,128]{2,1,0:T(8,128)} async-done(((f32[2,128,128]{2,1,0:T(8,128)}), f32[32,128,128]{2,1,0:T(8,128)}) %all-gather.8.cloned.1.call-update) | async-done | bytes 2097168 | tf_op jit(solution)/shard_map/all_gather | solution.py:43
  235.7 16.2 %while.25 = (s32[]{:T(128)}, f32[2,128]{1,0:T(2,128)S(1)}, f32[2,128,128]{2,1,0:T(8,128)S(1)}, s32[]{:T(128)}, f32[16,2,128]{2,1,0:T(2,128)S(1)}, /*index=5*/f32...) while((s32[]{:T(128)}, f32[2,128]{1,0:T(2,128)S(1)}, f32[2,128,128]{2,1,0:T(8,128)S(1)}, s32[]{:T(128)}, ...), condition=%wide.region_6.7_spmd, body=%wide.region_5.6_spmd.sunk | while | flops 65797 | bytes 398471 | solution.py:51
  235.7 1.0 bitcast_add_fusion.7
  236.8 1.0 bitcast_add_fusion.7
  237.9 1.0 bitcast_add_fusion.7
  239.0 1.0 bitcast_add_fusion.7
  242.2 1.0 bitcast_add_fusion.7
  243.3 1.0 bitcast_add_fusion.7
  247.6 1.0 bitcast_add_fusion.7
  248.6 1.0 bitcast_add_fusion.7
  253.1 1.7 fusion.19
  254.8 3.7 %fusion = bf16[256,2048]{1,0:T(8,128)(2,1)} fusion(f32[256,2048]{1,0:T(8,128)S(1)} %fusion.19, bf16[2048,1536]{1,0:T(8,128)(2,1)} %all-gather.6.cloned.1.call-done, f32[2,128]{0,1:T(8,128)S(1)} %collective-permute-done, f32[256,128]{0,1:T(8,128)S(1)} %fusion.15, bf16[256,2048]{1,0:T(8,128)(2,1)S(1)} %bitcast.116, f32[128]{0:T(128)S(1)} %get-tuple-element.133, ...), kind=kOutput, calls=%fused_computation.6 | convolution fusion | flops 269877248 | bytes 5377024 | tf_op jit(solution)/shard_map/dot_general | solution.py:216
  258.5 20.6 %all_to_all.10 = bf16[8,32,2048]{2,1,0:T(8,128)(2,1)S(1)} all-to-all(bf16[8,32,2048]{2,1,0:T(8,128)(2,1)} %bitcast.117), channel_id=1, replica_groups=mesh['sp'=16,'fs'=4,'tp'=8] {'tp'}, dimensions={0} | all-to-all | bytes 2097152 | tf_op jit(solution)/shard_map/all_to_all | solution.py:67
  (88 shorter events, 20.7 us)
Async XLA Ops:
  6.5 153.9 %all-gather.6.cloned.1.call-start = ((), (), s32[]{:S(2)}) async-start(), calls=%async_computation.2 | async-start | bytes 6389760 | tf_op jit(solution)/shard_map/all_gather | solution.py:15
  12.2 0.6 copy-start.1
  14.9 20.2 %all-to-all-start = ((bf16[8,32,2048]{2,1,0:T(8,128)(2,1)}), bf16[8,32,2048]{2,1,0:T(8,128)(2,1)S(1)}, u32[]{:S(2)}, u32[]{:S(2)}) async-start(bf16[8,32,2048]{2,1,0:T(8,128)(2,1)} %broadcast_in_dim.41), calls=%async_computation | async-start | bytes 2097152 | tf_op jit(solution)/shard_map/all_to_all | solution.py:27
  19.2 216.4 %all-gather.8.cloned.1.call-start = ((), (), s32[]{:S(2)}) async-start(), calls=%async_computation.3 | async-start | bytes 2228224 | tf_op jit(solution)/shard_map/all_gather | solution.py:43
  160.4 6.3 %copy-start.3 = (f32[3,128]{1,0:T(4,128)S(1)}, f32[3,128]{1,0:T(4,128)}, u32[]{:S(2)}) copy-start(f32[3,128]{1,0:T(4,128)} %param.30) | copy-start | bytes 4612
  165.9 0.7 copy-start
  165.9 85.9 %copy-start.2 = (f32[1,2,128,128]{3,2,1,0:T(8,128)S(1)}, f32[1,2,128,128]{3,2,1,0:T(8,128)}, u32[]{:S(2)}) copy-start(f32[1,2,128,128]{3,2,1,0:T(8,128)} %param.28) | copy-start | bytes 393220
  168.4 84.7 %copy-start.4 = (f32[256]{0:T(256)S(1)}, f32[256]{0:T(256)}, u32[]{:S(2)}) copy-start(f32[256]{0:T(256)} %param.29) | copy-start | bytes 3076
  172.0 82.8 %collective-permute-start = (f32[2,128]{0,1:T(8,128)S(1)}, f32[2,128]{0,1:T(8,128)S(1)}, u32[]{:S(2)}, u32[]{:S(2)}) collective-permute-start(f32[2,128]{0,1:T(8,128)S(1)} %slice.29), channel_id=1, source_target_pairs={{0,32},{32,64},{64,96},{96,128},{128,160},{160,192},{192,224},{224... | collective-permute-start | bytes 3080 | tf_op jit(solution)/shard_map/ppermute | solution.py:57
Sparse Core Ops, SparseCore 0:
  13.0 147.3 all-gather.5
  166.7 68.8 all-gather.7
where the time goes:
time: 288 us; the launch traced here: 287 us
  waiting for transfers between devices  175 us (61%)
  blocking collectives  48.5 us (17%)
  other arithmetic  17.6 us (6%)
  matrix products  14.6 us (5%)
  between operations  13.7 us (5%)
  local copies, waits for them, and re-layouts  11.5 us (4%)
  starting transfers between devices  5.63 us (2%)
    all_gather x1, waiting for transfers between devices, gather_turned(): result = lax.all_gather(both, axis, axis=0, tiled=True)  125 us
    all_gather x1, waiting for transfers between devices, carried_in(): gathered = jax.tree.map(lambda a: lax.all_gather(a, axis), part)  34.2 us
    all_gather x1, blocking collectives, carried_in(): gathered = jax.tree.map(lambda a: lax.all_gather(a, axis), part)  27.9 us
    all_to_all x1, blocking collectives, summed_on_arrival(): lax.all_to_all(parts, axis, split_axis=0, concat_axis=0, tiled=True)  20.6 us
    add x15, other arithmetic, chain_combine(): later_part[0][..., None] * earlier_part[1] + later_part[1]  15.4 us
    all_to_all x1, waiting for transfers between devices, copy_for_each(): return lax.all_to_all(copies, axis, split_axis=0, concat_axis=0, tiled=True)  15.1 us
    dot_general x5, matrix products, shards(): jnp.dot(block_rows, weight, preferred_element_type=jnp.float32)  8.2 us
    unnamed x18, local copies, waits for them, and re-layouts  6.28 us
  transfers between devices with their start and end apart: 4, of which 3 were waited for; matrix products, arithmetic and copies ran while one was open for 9% of the time, Pallas kernels for 0%

commit v1 on v0

--- a/solution.py
+++ b/solution.py
@@ -12,7 +12,9 @@
     turned = [jnp.moveaxis(a, dim, 0) for a, dim in zip(arrays, dims)]
     widths = [t[0].size for t in turned]
     both = jnp.concatenate([t.reshape(-1, w) for t, w in zip(turned, widths)], axis=1)
-    result = lax.all_gather(both, axis, axis=0, tiled=True)
+    result = jnp.concatenate(
+        lax.all_to_all(jnp.stack([both] * lax.axis_size(axis)), axis, 0, 0), axis=0
+    )
     parts = jnp.split(result, [sum(widths[:k]) for k in range(1, len(widths))], axis=1)
     return tuple(
         (

time: 288 us -> 445 us (1.55)
  the two profiles are of different devices: /device:TPU:488 before, /device:TPU:480 now
where the time goes in v1:
time: 445 us; the launch traced here: 444 us
  waiting for transfers between devices  311 us (70%)
  blocking collectives  53.9 us (12%)
  starting transfers between devices  18.2 us (4%)
  other arithmetic  17.6 us (4%)
  matrix products  14.7 us (3%)
  local copies, waits for them, and re-layouts  14.2 us (3%)
  between operations  13.7 us (3%)
    all_to_all x1, waiting for transfers between devices, gather_turned(): lax.all_to_all(jnp.stack([both] * lax.axis_size(axis)), axis, 0, 0)  272 us
    all_gather x1, blocking collectives, carried_in(): gathered = jax.tree.map(lambda a: lax.all_gather(a, axis), part)  33.1 us
    all_gather x1, waiting for transfers between devices, carried_in(): gathered = jax.tree.map(lambda a: lax.all_gather(a, axis), part)  28.8 us
    all_to_all x1, blocking collectives, summed_on_arrival(): lax.all_to_all(parts, axis, split_axis=0, concat_axis=0, tiled=True)  20.9 us
    add x15, other arithmetic, chain_combine(): later_part[0][..., None] * earlier_part[1] + later_part[1]  15.4 us
    all_to_all x1, starting transfers between devices, gather_turned(): lax.all_to_all(jnp.stack([both] * lax.axis_size(axis)), axis, 0, 0)  12.6 us
    all_to_all x1, waiting for transfers between devices, copy_for_each(): return lax.all_to_all(copies, axis, split_axis=0, concat_axis=0, tiled=True)  10.2 us
  transfers between devices with their start and end apart: 4, of which 3 were waited for; matrix products, arithmetic and copies ran while one was open for 7% of the time, Pallas kernels for 0%

profile of v1, /device:TPU:480, one launch (start us, length us, event | category | flops | bytes accessed | tf_op | source)
XLA Modules:
  0.0 444.0 jit_solution(13738647609879659848)
XLA Ops:
  6.5 2.0 broadcast_in_dim.41
  8.5 4.3 all-to-all-start.1
  18.5 10.2 %all-to-all-done.1 = bf16[8,32,2048]{2,1,0:T(8,128)(2,1)S(1)} async-done(((bf16[8,32,2048]{2,1,0:T(8,128)(2,1)}), bf16[8,32,2048]{2,1,0:T(8,128)(2,1)S(1)}, u32[]{:S(2)}, u32[]{:S(2)}) %all-to-all-start.1) | async-done | bytes 1048608 | tf_op jit(solution)/shard_map/all_to_all | solution.py:29
  28.8 3.4 stack.2
  32.2 12.6 %all-to-all-start = ((bf16[64,32,1536]{2,1,0:T(8,128)(2,1)}), bf16[64,32,1536]{2,1,0:T(8,128)(2,1)}, u32[]{:S(2)}, u32[]{:S(2)}) async-start(bf16[64,32,1536]{2,1,0:T(8,128)(2,1)} %stack.2), calls=%async_computation | async-start | bytes 12582912 | tf_op jit(solution)/shard_map/all_to_all | solution.py:16
  44.9 272.0 %all-to-all-done = bf16[64,32,1536]{2,1,0:T(8,128)(2,1)} async-done(((bf16[64,32,1536]{2,1,0:T(8,128)(2,1)}), bf16[64,32,1536]{2,1,0:T(8,128)(2,1)}, u32[]{:S(2)}, u32[]{:S(2)}) %all-to-all-start) | async-done | bytes 6291488 | tf_op jit(solution)/shard_map/all_to_all | solution.py:16
  317.0 1.7 fusion.12
  318.7 1.7 fusion.8
  323.2 1.7 fusion.11
  325.4 1.5 fusion.16
  326.9 1.5 fusion.15
  329.2 1.3 collective-permute-start
  330.5 33.1 %all-gather.2 = f32[16,2,128]{2,1,0:T(2,128)S(1)} all-gather(f32[1,2,128]{2,1,0:T(2,128)S(1)} %exponential_bitcast_fusion.1), channel_id=2, replica_groups=mesh['sp'=16,'fs'=4,'tp'=8] {'sp'}, dimensions={0}, use_global_device_ids=true | all-gather | bytes 17408 | tf_op jit(solution)/shard_map/all_gather | solution.py:45
  363.9 28.8 %all-gather.5.cloned.1.call-done = f32[32,128,128]{2,1,0:T(8,128)} async-done(((f32[2,128,128]{2,1,0:T(8,128)}), f32[32,128,128]{2,1,0:T(8,128)}) %all-gather.5.cloned.1.call-update) | async-done | bytes 2097168 | tf_op jit(solution)/shard_map/all_gather | solution.py:45
  392.6 16.2 %while.25 = (s32[]{:T(128)}, f32[2,128]{1,0:T(2,128)S(1)}, f32[2,128,128]{2,1,0:T(8,128)S(1)}, s32[]{:T(128)}, f32[16,2,128]{2,1,0:T(2,128)S(1)}, /*index=5*/f32...) while((s32[]{:T(128)}, f32[2,128]{1,0:T(2,128)S(1)}, f32[2,128,128]{2,1,0:T(8,128)S(1)}, s32[]{:T(128)}, ...), condition=%wide.region_6.7_spmd, body=%wide.region_5.6_spmd.sunk | while | flops 65797 | bytes 398471 | solution.py:53
  392.7 1.0 bitcast_add_fusion.7
  397.0 1.0 bitcast_add_fusion.7
  398.1 1.0 bitcast_add_fusion.7
  401.3 1.0 bitcast_add_fusion.7
  402.4 1.0 bitcast_add_fusion.7
  403.4 1.0 bitcast_add_fusion.7
  410.1 1.7 fusion.19
  411.8 3.7 fusion
  415.5 20.9 %all_to_all.15 = bf16[8,32,2048]{2,1,0:T(8,128)(2,1)S(1)} all-to-all(bf16[8,32,2048]{2,1,0:T(8,128)(2,1)} %bitcast.118), channel_id=1, replica_groups=mesh['sp'=16,'fs'=4,'tp'=8] {'tp'}, dimensions={0} | all-to-all | bytes 2097152 | tf_op jit(solution)/shard_map/all_to_all | solution.py:69
  (90 shorter events, 22.1 us)
Async XLA Ops:
  8.5 20.2 %all-to-all-start.1 = ((bf16[8,32,2048]{2,1,0:T(8,128)(2,1)}), bf16[8,32,2048]{2,1,0:T(8,128)(2,1)S(1)}, u32[]{:S(2)}, u32[]{:S(2)}) async-start(bf16[8,32,2048]{2,1,0:T(8,128)(2,1)} %broadcast_in_dim.41), calls=%async_computation.1 | async-start | bytes 2097152 | tf_op jit(solution)/shard_map/all_to_all | solution.py:29
  32.2 12.7 %copy-start.2 = (f32[1,2,256]{2,1,0:T(2,128)S(1)}, f32[1,2,256]{2,1,0:T(2,128)}, u32[]{:S(2)}) copy-start(f32[1,2,256]{2,1,0:T(2,128)} %param.27) | copy-start | bytes 6148
  32.2 286.5 %copy-start.5 = (f32[256]{0:T(256)S(1)}, f32[256]{0:T(256)}, u32[]{:S(2)}) copy-start(f32[256]{0:T(256)} %param.26) | copy-start | bytes 3076
  32.2 284.8 %all-to-all-start = ((bf16[64,32,1536]{2,1,0:T(8,128)(2,1)}), bf16[64,32,1536]{2,1,0:T(8,128)(2,1)}, u32[]{:S(2)}, u32[]{:S(2)}) async-start(bf16[64,32,1536]{2,1,0:T(8,128)(2,1)} %stack.2), calls=%async_computation | async-start | bytes 12582912 | tf_op jit(solution)/shard_map/all_to_all | solution.py:16
  44.8 347.8 %all-gather.5.cloned.1.call-start = ((), (), s32[]{:S(2)}) async-start(), calls=%async_computation.3 | async-start | bytes 2228224 | tf_op jit(solution)/shard_map/all_gather | solution.py:45
  318.7 4.5 %copy-start.3 = (f32[3,128]{1,0:T(4,128)S(1)}, f32[3,128]{1,0:T(4,128)}, u32[]{:S(2)}) copy-start(f32[3,128]{1,0:T(4,128)} %param.30) | copy-start | bytes 4612
  322.5 0.7 copy-start
  322.5 86.3 %copy-start.1 = (f32[1,2,128,128]{3,2,1,0:T(8,128)S(1)}, f32[1,2,128,128]{3,2,1,0:T(8,128)}, u32[]{:S(2)}) copy-start(f32[1,2,128,128]{3,2,1,0:T(8,128)} %param.28) | copy-start | bytes 393220
  325.0 85.1 %copy-start.4 = (f32[256]{0:T(256)S(1)}, f32[256]{0:T(256)}, u32[]{:S(2)}) copy-start(f32[256]{0:T(256)} %param.29) | copy-start | bytes 3076
  329.2 82.6 %collective-permute-start = (f32[2,128]{0,1:T(8,128)}, f32[2,128]{0,1:T(8,128)}, u32[]{:S(2)}, u32[]{:S(2)}) collective-permute-start(f32[2,128]{0,1:T(8,128)} %slice.29), channel_id=1, source_target_pairs={{0,32},{32,64},{64,96},{96,128},{128,160},{160,192},{192,224},{224... | collective-permute-start | bytes 3080 | tf_op jit(solution)/shard_map/ppermute | solution.py:59
Sparse Core Ops, SparseCore 0:
  323.3 69.2 all-gather.4
